TPU v7x, 32 devices: a whole 2x2x4 slice. The times are simulated.
32 devices in a mesh: grp: 2 (over y), ep: 8 (over z, x), tp: 2 (over core).
Axes of the slice: x: 2, y: 2, z: 4, core: 2. Of those that a mesh axis runs over, the one named last changes fastest.
Arguments:
- tokens: bfloat16 [384, 2048], P(('grp', 'ep')), parts along dimension 0, may hold values from -6 to 6
- norm_gain: float32 [2048], replicated, may hold values from 0.1 to 1.9
- routes: int32 [384, 4], P(('grp', 'ep')), parts along dimension 0, may hold values from 0 to 7, all different within a row; in each aligned block of 24 rows (0 to 23, 24 to 47, ...) at most 24 rows name the same one
- gate_scores: float32 [384, 4], P(('grp', 'ep')), parts along dimension 0, may hold values from 0.05 to 1
- w_gate: bfloat16 [8, 2048, 512], P('ep', None, 'tp'), may hold values from -1 to 1
- w_up: bfloat16 [8, 2048, 512], P('ep', None, 'tp'), may hold values from -1 to 1
- w_down: bfloat16 [8, 512, 2048], P('ep', 'tp'), may hold values from -0.0625 to 0.0625
Outputs:
- mixed: bfloat16 [384, 2048], P(('grp', 'ep')), parts along dimension 0
There are 2 independent parts, one for each index of `grp`. A program takes and returns all parts, laid end to end along the dimension named above; an argument that names none is the same for every part. Nothing has to cross between parts.
Inputs may be any that keep to these rules, and one draw needn't show every extreme that they name: `routes`: each row names 4 different experts; among the 24 rows of one device no expert is named more than 24 times, a bound that some block reaches.
All inputs are finite; a program needn't handle non-finite values.
Results may differ from a plain program's by a relative error of at most 0.0077.
Values may be sent and summed in bfloat16 or wider, within the bound.
No kernel may reach another device: no remote copies, remote signals or barrier semaphores. Data moves between devices by JAX's collectives and lax.ppermute only.
A program may use at most 64 MiB of HBM per device.

v0:
```python
import jax
import jax.numpy as jnp
from jax import lax
from jax.sharding import PartitionSpec as P


def clamped_unit(g, u):
    gate = jnp.minimum(g, 7.0)
    up = jnp.clip(u, -7.0, 7.0)
    return (up + 1.0) * gate * jax.nn.sigmoid(1.702 * gate)


def expert_rows(rows, wg, wu, wd):
    g = jnp.dot(rows, wg, preferred_element_type=jnp.float32)
    u = jnp.dot(rows, wu, preferred_element_type=jnp.float32)
    act = clamped_unit(g, u).astype(jnp.bfloat16)
    part = jnp.dot(act, wd, preferred_element_type=jnp.float32)
    part = lax.optimization_barrier(part.astype(jnp.bfloat16)).astype(jnp.float32)
    total = lax.psum(part.astype(jnp.bfloat16), "tp")
    return total


def finish(mixed):
    result = mixed.astype(jnp.bfloat16)
    return result


def slot_table(routes, scores, experts, capacity):
    count = routes.shape[0]
    chosen = routes[:, :, None] == experts[None, None, :]
    hit = jnp.any(chosen, axis=1).astype(jnp.int32)
    weight = jnp.sum(jnp.where(chosen, scores[:, :, None], 0.0), axis=1)
    rank = jnp.cumsum(hit, axis=0) - hit
    places = jnp.arange(capacity, dtype=jnp.int32)
    match = (hit[:, :, None] == 1) & (rank[:, :, None] == places[None, None, :])
    row_ids = jnp.arange(count, dtype=jnp.int32)[:, None, None]
    filled = jnp.any(match, axis=0)
    slot_tok = jnp.sum(jnp.where(match, row_ids, 0), axis=0) + count * (
        1 - filled.astype(jnp.int32)
    )
    slot_w = jnp.sum(jnp.where(match, weight[:, :, None], 0.0), axis=0)
    return (slot_tok, slot_w)


def body(tokens, norm_gain, routes, gate_scores, w_gate, w_up, w_down):
    count, width = tokens.shape
    top = routes.shape[1]
    nexp = lax.axis_size("ep")
    capacity = max(2, min(count, 2 * count * top // nexp))
    wg, wu, wd = (w_gate[0], w_up[0], w_down[0])
    xf = tokens.astype(jnp.float32)
    normed = (xf * lax.rsqrt(jnp.mean(xf * xf, axis=-1, keepdims=True) + 1e-06) * norm_gain).astype(
        jnp.bfloat16
    )
    experts = jnp.arange(nexp, dtype=jnp.int32)
    slot_tok, slot_w = slot_table(routes, gate_scores, experts, capacity)
    padded = jnp.concatenate([normed, jnp.zeros((1, width), jnp.bfloat16)], axis=0)
    outgoing = padded[slot_tok]
    received = lax.all_to_all(outgoing, "ep", split_axis=0, concat_axis=0, tiled=True)
    sources, places, _ = received.shape
    outputs = expert_rows(received.reshape(sources * places, width), wg, wu, wd)
    returned = lax.all_to_all(
        outputs.reshape(sources, places, outputs.shape[1]),
        "ep",
        split_axis=0,
        concat_axis=0,
        tiled=True,
    )
    flat_tok = slot_tok.reshape(-1)
    token_ids = jnp.arange(count, dtype=jnp.int32)
    combine = jnp.where(flat_tok[None, :] == token_ids[:, None], slot_w.reshape(-1)[None, :], 0.0)
    mixed = jnp.dot(
        combine,
        returned.reshape(-1, returned.shape[2]).astype(jnp.float32),
        precision=lax.Precision.HIGHEST,
    )
    return finish(mixed)


def solution(mesh):
    in_specs = (
        P(("grp", "ep"), None),
        P(),
        P(("grp", "ep"), None),
        P(("grp", "ep"), None),
        P("ep", None, "tp"),
        P("ep", None, "tp"),
        P("ep", "tp", None),
    )
    out_specs = P(("grp", "ep"), None)
    return jax.shard_map(body, mesh=mesh, in_specs=in_specs, out_specs=out_specs, check_vma=False)
```

profile of v0, /device:TPU:0, one launch (start us, length us, event | category | flops | bytes accessed | tf_op | source)
XLA Modules:
  0.0 94.1 jit_solution(17916535765891462060)
XLA Ops:
  6.5 0.0 copy-start
  6.5 0.0 all-reduce.3.cloned.1.call-start
  6.5 0.8 fusion.23
  7.3 0.1 copy.10
  7.5 0.1 fusion.21
  7.6 0.1 select_reduce_fusion.1
  7.7 1.0 %fusion.8 = f32[24]{0:T(128)S(1)} fusion(bf16[24,2048]{1,0:T(8,128)(2,1)} %param.7), kind=kLoop, calls=%fused_computation.14 | loop fusion | flops 147432 | bytes 98400 | tf_op jit(solution)/shard_map/reduce_sum | solution.py:52
  8.8 0.1 reshape.96
  8.9 1.0 %fusion.10 = bf16[24,2048]{1,0:T(8,128)(2,1)S(1)} fusion(bf16[24,2048]{1,0:T(8,128)(2,1)} %param.7, f32[2048]{0:T(1024)} %param.8, f32[24]{0:T(128)S(1)} %add_rsqrt_fusion), kind=kLoop, calls=%fused_computation.16 | loop fusion | flops 196608 | bytes 204896 | tf_op jit(solution)/shard_map/convert_element_type | solution.py:52
  9.9 1.1 %gather_fusion = bf16[192,2048]{1,0:T(8,128)(2,1)S(1)} fusion(bf16[25,2048]{1,0:T(8,128)(2,1)S(1)} %concatenate.3, s32[1024]{0:T(1024)S(1)} %pad_clamp_fusion), kind=kCustom, calls=%fused_computation | custom fusion | bytes 1573632 | tf_op jit(solution)/shard_map/gather | solution.py:58
  11.0 0.0 copy-start.1
  11.0 27.4 %all_to_all.10 = bf16[8,24,2048]{2,1,0:T(8,128)(2,1)S(1)} all-to-all(bf16[8,24,2048]{2,1,0:T(8,128)(2,1)S(1)} %bitcast.23), channel_id=1, replica_groups=mesh['grp'=2,'ep'=8,'tp'=2] {'ep'}, dimensions={0} | all-to-all | bytes 1572864 | tf_op jit(solution)/shard_map/all_to_all | solution.py:59
  38.4 0.0 copy-start.2
  38.4 0.0 copy-done.1
  38.4 0.4 convolution_minimum_fusion
  38.8 0.0 copy-done
  38.8 0.8 copy-done.2
  39.6 1.9 %convolution_convert_fusion = bf16[192,2048]{1,0:T(8,128)(2,1)} fusion(f32[192,256]{1,0:T(8,128)S(1)} %convolution_minimum_fusion, bf16[192,2048]{1,0:T(8,128)(2,1)S(1)} %bitcast.22, bf16[1,256,2048]{2,1,0:T(8,128)(2,1)S(1)} %copy-done, bf16[1,2048,256]{2,1,0:T(8,128)(2,1)S(1)} %copy-done.2), kind=kOutput, calls=%fused_computation.1 | convolution fusion | flops 403488768 | bytes 3866624 | tf_op jit(solution)/shard_map/dot_general | solution.py:17
  41.6 0.0 copy-start.3
  41.6 0.0 copy-start.4
  41.6 0.0 all-reduce.3.cloned.1.call-update
  41.6 18.2 %all-reduce.3.cloned.1.call-done = bf16[8,24,2048]{2,1,0:T(8,128)(2,1)} async-done(((bf16[8,24,2048]{2,1,0:T(8,128)(2,1)}), bf16[8,24,2048]{2,1,0:T(8,128)(2,1)}) %all-reduce.3.cloned.1.call-update) | async-done | bytes 786448 | tf_op jit(solution)/shard_map/psum | solution.py:19
  59.8 5.8 %all-to-all-start.1 = ((bf16[8,24,2048]{2,1,0:T(8,128)(2,1)}), bf16[8,24,2048]{2,1,0:T(8,128)(2,1)S(1)}, u32[]{:S(2)}, u32[]{:S(2)}) async-start(bf16[8,24,2048]{2,1,0:T(8,128)(2,1)} %all-reduce.3.cloned.1.call-done), calls=%async_computation.1 | async-start | bytes 1572864 | tf_op jit(solution)/shard_map/all_to_all | solution.py:62
  65.6 0.0 copy-done.3
  65.6 0.0 copy-done.4
  65.6 0.1 copy.11
  65.7 0.1 select_reduce_fusion
  65.8 0.1 broadcast_in_dim.69
  65.9 0.1 add.52
  66.0 20.2 %all-to-all-done.1 = bf16[8,24,2048]{2,1,0:T(8,128)(2,1)S(1)} async-done(((bf16[8,24,2048]{2,1,0:T(8,128)(2,1)}), bf16[8,24,2048]{2,1,0:T(8,128)(2,1)S(1)}, u32[]{:S(2)}, u32[]{:S(2)}) %all-to-all-start.1) | async-done | bytes 786464 | tf_op jit(solution)/shard_map/all_to_all | solution.py:62
  86.1 1.1 %convolution_convert_fusion.1 = bf16[24,2048]{1,0:T(8,128)(2,1)} fusion(bf16[192,2048]{1,0:T(8,128)(2,1)S(1)} %bitcast.24, f32[192]{0:T(256)S(1)} %broadcast_in_dim.69, s32[192]{0:T(256)S(1)} %add.52), kind=kOutput, calls=%fused_computation.2 | convolution fusion | flops 113304576 | bytes 886272 | tf_op jit(solution)/shard_map/dot_general | solution.py:72
  (8 shorter events, 0.1 us)
Async XLA Ops:
  6.5 32.3 %copy-start = (bf16[1,256,2048]{2,1,0:T(8,128)(2,1)S(1)}, bf16[1,256,2048]{2,1,0:T(8,128)(2,1)}, u32[]{:S(2)}) copy-start(bf16[1,256,2048]{2,1,0:T(8,128)(2,1)} %param.13) | copy-start | bytes 3145732
  6.5 53.2 %all-reduce.3.cloned.1.call-start = ((), (), s32[]{:S(2)}) async-start(), calls=%async_computation.2 | async-start | bytes 1572864 | tf_op jit(solution)/shard_map/psum | solution.py:19
  11.0 27.4 %copy-start.1 = (bf16[1,2048,256]{2,1,0:T(8,128)(2,1)S(1)}, bf16[1,2048,256]{2,1,0:T(8,128)(2,1)}, u32[]{:S(2)}) copy-start(bf16[1,2048,256]{2,1,0:T(8,128)(2,1)} %param.11) | copy-start | bytes 3145732
  38.4 1.2 %copy-start.2 = (bf16[1,2048,256]{2,1,0:T(8,128)(2,1)S(1)}, bf16[1,2048,256]{2,1,0:T(8,128)(2,1)}, u32[]{:S(2)}) copy-start(bf16[1,2048,256]{2,1,0:T(8,128)(2,1)} %param.12) | copy-start | bytes 3145732
  41.6 24.0 %copy-start.3 = (s32[24,4]{0,1:T(4,128)S(1)}, s32[24,4]{0,1:T(4,128)}, u32[]{:S(2)}) copy-start(s32[24,4]{0,1:T(4,128)} %param.9) | copy-start | bytes 1156
  41.6 24.0 %copy-start.4 = (f32[24,4]{0,1:T(4,128)S(1)}, f32[24,4]{0,1:T(4,128)}, u32[]{:S(2)}) copy-start(f32[24,4]{0,1:T(4,128)} %param.10) | copy-start | bytes 1156
  59.8 26.4 %all-to-all-start.1 = ((bf16[8,24,2048]{2,1,0:T(8,128)(2,1)}), bf16[8,24,2048]{2,1,0:T(8,128)(2,1)S(1)}, u32[]{:S(2)}, u32[]{:S(2)}) async-start(bf16[8,24,2048]{2,1,0:T(8,128)(2,1)} %all-reduce.3.cloned.1.call-done), calls=%async_computation.1 | async-start | bytes 1572864 | tf_op jit(solution)/shard_map/all_to_all | solution.py:62
Sparse Core Ops, SparseCore 0:
  41.7 17.9 all-reduce.2
where the time goes:
time: 94.4 us; the launch traced here: 94.1 us
  waiting for transfers between devices  38.3 us (41%)
  blocking collectives  27.4 us (29%)
  between operations  13.5 us (14%)
  starting transfers between devices  5.81 us (6%)
  matrix products  3.4 us (4%)
  other arithmetic  3.26 us (3%)
  local copies, waits for them, and re-layouts  2.39 us (3%)
    all_to_all x1, blocking collectives, body(): lax.all_to_all(outgoing, 'ep', split_axis=0, concat_axis=0, tiled=True)  27.4 us
    all_to_all x1, waiting for transfers between devices, body(): lax.all_to_all(outputs.reshape(sources, places, outputs.shape[1]), 'ep',...  20.2 us
    psum x1, waiting for transfers between devices, expert_rows(): total = lax.psum(part.astype(jnp.bfloat16), 'tp')  18.2 us
    all_to_all x1, starting transfers between devices, body(): lax.all_to_all(outputs.reshape(sources, places, outputs.shape[1]), 'ep',...  5.81 us
    dot_general x1, matrix products, expert_rows(): part = jnp.dot(act, wd, preferred_element_type=jnp.float32)  1.94 us
  transfers between devices with their start and end apart: 2, of which 2 were waited for; matrix products, arithmetic and copies ran while one was open for 0% of the time, Pallas kernels for 0%

commit v1 on v0

--- a/solution.py
+++ b/solution.py
@@ -2,6 +2,11 @@
 import jax.numpy as jnp
 from jax import lax
 from jax.sharding import PartitionSpec as P
+
+
+def gather_and_add(x, axis):
+    pieces = lax.all_gather(x, axis)
+    return jnp.sum(pieces, axis=0)
 
 
 def clamped_unit(g, u):
@@ -16,7 +21,7 @@
     act = clamped_unit(g, u).astype(jnp.bfloat16)
     part = jnp.dot(act, wd, preferred_element_type=jnp.float32)
     part = lax.optimization_barrier(part.astype(jnp.bfloat16)).astype(jnp.float32)
-    total = lax.psum(part.astype(jnp.bfloat16), "tp")
+    total = gather_and_add(part.astype(jnp.bfloat16), "tp")
     return total
 
 

time: 94.4 us -> 88.1 us (0.933)
  waiting for transfers between devices: 38.3 us -> 29.2 us
  other arithmetic: 3.26 us -> 6.1 us
    psum x1 -> x0, waiting for transfers between devices: 18.2 us -> none  [expert_rows(): total = lax.psum(part.astype(jnp.bfloat16), 'tp')]
    all_gather x0 -> x1, waiting for transfers between devices: none -> 8.99 us  [gather_and_add(): pieces = lax.all_gather(x, axis)]
    reduce_sum x0 -> x1, other arithmetic: none -> 2.83 us  [gather_and_add(): return jnp.sum(pieces, axis=0)]
where the time goes in v1:
time: 88.1 us; the launch traced here: 87.7 us
  waiting for transfers between devices  29.2 us (33%)
  blocking collectives  27.4 us (31%)
  between operations  13.5 us (15%)
  other arithmetic  6.1 us (7%)
  starting transfers between devices  5.78 us (7%)
  matrix products  3.39 us (4%)
  local copies, waits for them, and re-layouts  2.38 us (3%)
    all_to_all x1, blocking collectives, body(): lax.all_to_all(outgoing, 'ep', split_axis=0, concat_axis=0, tiled=True)  27.4 us
    all_to_all x1, waiting for transfers between devices, body(): lax.all_to_all(outputs.reshape(sources, places, outputs.shape[1]), 'ep',...  20.2 us
    all_gather x1, waiting for transfers between devices, gather_and_add(): pieces = lax.all_gather(x, axis)  8.99 us
    all_to_all x1, starting transfers between devices, body(): lax.all_to_all(outputs.reshape(sources, places, outputs.shape[1]), 'ep',...  5.78 us
    reduce_sum x1, other arithmetic, gather_and_add(): return jnp.sum(pieces, axis=0)  2.83 us
    dot_general x1, matrix products, expert_rows(): part = jnp.dot(act, wd, preferred_element_type=jnp.float32)  1.93 us
  transfers between devices with their start and end apart: 2, of which 2 were waited for; matrix products, arithmetic and copies ran while one was open for 0% of the time, Pallas kernels for 0%

profile of v1, /device:TPU:0, one launch (start us, length us, event | category | flops | bytes accessed | tf_op | source)
XLA Modules:
  0.0 87.7 jit_solution(7622431958103664555)
XLA Ops:
  6.5 0.0 copy-start
  6.5 0.0 all-gather.3.cloned.1.call-start
  6.5 0.8 fusion.23
  7.3 0.1 copy.10
  7.5 0.1 fusion.21
  7.6 0.1 select_reduce_fusion.1
  7.7 1.0 %fusion.8 = f32[24]{0:T(128)S(1)} fusion(bf16[24,2048]{1,0:T(8,128)(2,1)} %param.7), kind=kLoop, calls=%fused_computation.14 | loop fusion | flops 147432 | bytes 98400 | tf_op jit(solution)/shard_map/reduce_sum | solution.py:57
  8.8 0.1 reshape.96
  8.9 1.0 %fusion.10 = bf16[24,2048]{1,0:T(8,128)(2,1)S(1)} fusion(bf16[24,2048]{1,0:T(8,128)(2,1)} %param.7, f32[2048]{0:T(1024)} %param.8, f32[24]{0:T(128)S(1)} %add_rsqrt_fusion), kind=kLoop, calls=%fused_computation.16 | loop fusion | flops 196608 | bytes 204896 | tf_op jit(solution)/shard_map/convert_element_type | solution.py:57
  9.9 1.1 %gather_fusion = bf16[192,2048]{1,0:T(8,128)(2,1)S(1)} fusion(bf16[25,2048]{1,0:T(8,128)(2,1)S(1)} %concatenate.3, s32[1024]{0:T(1024)S(1)} %pad_clamp_fusion), kind=kCustom, calls=%fused_computation | custom fusion | bytes 1573632 | tf_op jit(solution)/shard_map/gather | solution.py:63
  11.0 0.0 copy-start.1
  11.0 27.4 %all_to_all.10 = bf16[8,24,2048]{2,1,0:T(8,128)(2,1)S(1)} all-to-all(bf16[8,24,2048]{2,1,0:T(8,128)(2,1)S(1)} %bitcast.24), channel_id=1, replica_groups=mesh['grp'=2,'ep'=8,'tp'=2] {'ep'}, dimensions={0} | all-to-all | bytes 1572864 | tf_op jit(solution)/shard_map/all_to_all | solution.py:64
  38.4 0.0 copy-start.2
  38.4 0.0 copy-done.1
  38.4 0.4 convolution_minimum_fusion
  38.8 0.0 copy-done
  38.8 0.8 copy-done.2
  39.6 1.9 %convolution_convert_fusion = bf16[192,2048]{1,0:T(8,128)(2,1)} fusion(f32[192,256]{1,0:T(8,128)S(1)} %convolution_minimum_fusion, bf16[192,2048]{1,0:T(8,128)(2,1)S(1)} %bitcast.23, bf16[1,256,2048]{2,1,0:T(8,128)(2,1)S(1)} %copy-done, bf16[1,2048,256]{2,1,0:T(8,128)(2,1)S(1)} %copy-done.2), kind=kOutput, calls=%fused_computation.1 | convolution fusion | flops 403488768 | bytes 3866624 | tf_op jit(solution)/shard_map/dot_general | solution.py:22
  41.6 0.0 all-gather.3.cloned.1.call-update
  41.6 9.0 %all-gather.3.cloned.1.call-done = bf16[384,2048]{1,0:T(8,128)(2,1)} async-done(((bf16[192,2048]{1,0:T(8,128)(2,1)}), bf16[384,2048]{1,0:T(8,128)(2,1)}) %all-gather.3.cloned.1.call-update) | async-done | bytes 1572880 | tf_op jit(solution)/shard_map/all_gather | solution.py:8
  50.6 0.0 copy-start.3
  50.6 0.0 copy-start.4
  50.6 2.8 %reduce_sum.52 = bf16[192,2048]{1,0:T(8,128)(2,1)} reduce(bf16[2,192,2048]{2,1,0:T(8,128)(2,1)} %bitcast.26, bf16[]{:T(256)} %constant.8.clone.1), dimensions={0}, to_apply=%region_7.8 | reduce | flops 393216 | bytes 2359298 | tf_op jit(solution)/shard_map/reduce_sum | solution.py:9
  53.4 5.8 %all-to-all-start.1 = ((bf16[8,24,2048]{2,1,0:T(8,128)(2,1)}), bf16[8,24,2048]{2,1,0:T(8,128)(2,1)S(1)}, u32[]{:S(2)}, u32[]{:S(2)}) async-start(bf16[8,24,2048]{2,1,0:T(8,128)(2,1)} %bitcast.7), calls=%async_computation.1 | async-start | bytes 1572864 | tf_op jit(solution)/shard_map/all_to_all | solution.py:67
  59.2 0.0 copy-done.3
  59.2 0.0 copy-done.4
  59.2 0.1 copy.11
  59.3 0.1 select_reduce_fusion
  59.4 0.1 broadcast_in_dim.69
  59.5 0.1 add.50
  59.6 20.2 %all-to-all-done.1 = bf16[8,24,2048]{2,1,0:T(8,128)(2,1)S(1)} async-done(((bf16[8,24,2048]{2,1,0:T(8,128)(2,1)}), bf16[8,24,2048]{2,1,0:T(8,128)(2,1)S(1)}, u32[]{:S(2)}, u32[]{:S(2)}) %all-to-all-start.1) | async-done | bytes 786464 | tf_op jit(solution)/shard_map/all_to_all | solution.py:67
  79.8 1.1 %convolution_convert_fusion.1 = bf16[24,2048]{1,0:T(8,128)(2,1)} fusion(bf16[192,2048]{1,0:T(8,128)(2,1)S(1)} %bitcast.25, f32[192]{0:T(256)S(1)} %broadcast_in_dim.69, s32[192]{0:T(256)S(1)} %add.50), kind=kOutput, calls=%fused_computation.2 | convolution fusion | flops 113304576 | bytes 886272 | tf_op jit(solution)/shard_map/dot_general | solution.py:77
  (8 shorter events, 0.1 us)
Async XLA Ops:
  6.5 32.3 %copy-start = (bf16[1,256,2048]{2,1,0:T(8,128)(2,1)S(1)}, bf16[1,256,2048]{2,1,0:T(8,128)(2,1)}, u32[]{:S(2)}) copy-start(bf16[1,256,2048]{2,1,0:T(8,128)(2,1)} %param.13) | copy-start | bytes 3145732
  6.5 44.0 %all-gather.3.cloned.1.call-start = ((), (), s32[]{:S(2)}) async-start(), calls=%async_computation.2 | async-start | bytes 2359296 | tf_op jit(solution)/shard_map/all_gather | solution.py:8
  11.0 27.4 %copy-start.1 = (bf16[1,2048,256]{2,1,0:T(8,128)(2,1)S(1)}, bf16[1,2048,256]{2,1,0:T(8,128)(2,1)}, u32[]{:S(2)}) copy-start(bf16[1,2048,256]{2,1,0:T(8,128)(2,1)} %param.11) | copy-start | bytes 3145732
  38.4 1.2 %copy-start.2 = (bf16[1,2048,256]{2,1,0:T(8,128)(2,1)S(1)}, bf16[1,2048,256]{2,1,0:T(8,128)(2,1)}, u32[]{:S(2)}) copy-start(bf16[1,2048,256]{2,1,0:T(8,128)(2,1)} %param.12) | copy-start | bytes 3145732
  50.6 8.6 %copy-start.3 = (s32[24,4]{0,1:T(4,128)S(1)}, s32[24,4]{0,1:T(4,128)}, u32[]{:S(2)}) copy-start(s32[24,4]{0,1:T(4,128)} %param.9) | copy-start | bytes 1156
  50.6 8.6 %copy-start.4 = (f32[24,4]{0,1:T(4,128)S(1)}, f32[24,4]{0,1:T(4,128)}, u32[]{:S(2)}) copy-start(f32[24,4]{0,1:T(4,128)} %param.10) | copy-start | bytes 1156
  53.4 26.4 %all-to-all-start.1 = ((bf16[8,24,2048]{2,1,0:T(8,128)(2,1)}), bf16[8,24,2048]{2,1,0:T(8,128)(2,1)S(1)}, u32[]{:S(2)}, u32[]{:S(2)}) async-start(bf16[8,24,2048]{2,1,0:T(8,128)(2,1)} %bitcast.7), calls=%async_computation.1 | async-start | bytes 1572864 | tf_op jit(solution)/shard_map/all_to_all | solution.py:67
Sparse Core Ops, SparseCore 0:
  41.7 8.8 all-gather.2
